TPU v7x, 32 devices: a whole 2x2x4 slice. The times are simulated.
32 devices in a mesh: kv: 4 (over y, x), tp: 8 (over z, core).
Axes of the slice: x: 2, y: 2, z: 4, core: 2. Of those that a mesh axis runs over, the one named last changes fastest.
Arguments:
- tokens: bfloat16 [3, 4096], P(None, ('kv', 'tp')), may hold values from -40 to 40
- lengths: int32 [3], replicated, may hold values from 1 to 8192, as said below
- attn_gain: float32 [4096], P(('kv', 'tp')), may hold values from 0.1 to 1.9
- w_query: bfloat16 [4096, 2048], P('kv', 'tp'), may hold values from -0.09375 to 0.09375
- w_key: bfloat16 [4096, 128], P('kv'), may hold values from -0.09375 to 0.09375
- w_value: bfloat16 [4096, 128], P('kv'), may hold values from -0.09375 to 0.09375
- w_forget: bfloat16 [4096, 32], replicated, may hold values from -0.09375 to 0.09375
- forget_bias: float32 [32], replicated, may hold values from -4 to 0
- cache_keys: bfloat16 [3, 128, 8192], P(None, None, ('kv', 'tp')), may hold values from -320 to 320
- cache_values: bfloat16 [3, 128, 8192], P(None, None, ('kv', 'tp')), may hold values from -6 to 6
- cache_decay: float32 [3, 32, 8192], P(None, None, ('kv', 'tp')), may hold values from -1028 to 0, as said below
- out_gain: float32 [2048], replicated, may hold values from 0.1 to 1.9
- w_out: bfloat16 [2048, 4096], P('tp', 'kv'), may hold values from -0.125 to 0.125
- mlp_gain: float32 [4096], P(('kv', 'tp')), may hold values from 0.1 to 1.9
- w_gate: bfloat16 [4096, 11264], P('kv', 'tp'), may hold values from -0.09375 to 0.09375
- w_up: bfloat16 [4096, 11264], P('kv', 'tp'), may hold values from -0.09375 to 0.09375
- w_down: bfloat16 [11264, 4096], P('tp', 'kv'), may hold values from -0.0546875 to 0.0546875
Outputs:
- layer_out: bfloat16 [3, 4096], P(None, ('kv', 'tp'))
Inputs may be any that keep to these rules, and one draw needn't show every extreme that they name: Sequence b has lengths[b] live cache positions, 0 to lengths[b] - 1; some sequence has exactly 8192 in every draw. On live positions, cache_decay[b, h, j] is the sum of the log forget gates of sequence b and head h over positions j + 1 to lengths[b] - 1, so it is zero at the last live position and never rises toward earlier positions; it is zero beyond lengths[b].
All inputs are finite; a program needn't handle non-finite values.
Results may differ from a plain program's by a relative error of at most 0.013.
Values may be sent and summed in bfloat16 or wider, within the bound.
A program may use at most 64 MiB of HBM per device.

v0:
```python
import jax
import jax.numpy as jnp
from jax import lax
from jax.sharding import PartitionSpec as P

QUERY_HEAD_COUNT = 32
HD = 64
KV_HEADS = 2
epsilon = 1e-06
masked_score = -1e30


def spread_rows(share, gain):
    scaled = (share.astype(jnp.float32) * gain).astype(jnp.bfloat16)
    squares = jnp.sum(jnp.square(share.astype(jnp.float32)), axis=1)
    row_block = lax.all_gather(scaled, "tp", axis=1, tiled=True)
    square_total = lax.psum(squares, ("kv", "tp"))
    return (row_block, square_total)


def body(
    tokens,
    lengths,
    attn_gain,
    w_query,
    w_key,
    w_value,
    w_forget,
    forget_bias,
    cache_keys,
    cache_values,
    cache_decay,
    out_gain,
    w_out,
    mlp_gain,
    w_gate,
    w_up,
    w_down,
):
    full_width = tokens.shape[1] * lax.axis_size("kv") * lax.axis_size("tp")
    kv_index = lax.axis_index("kv")
    tp_index = lax.axis_index("tp")
    row_block, square_total = spread_rows(tokens, attn_gain)
    block_rows = row_block.shape[1]
    forget_rows = lax.dynamic_slice_in_dim(w_forget, kv_index * block_rows, block_rows, 0)
    query_part = jnp.dot(row_block, w_query, preferred_element_type=jnp.float32)
    key_part = jnp.dot(row_block, w_key, preferred_element_type=jnp.float32)
    value_part = jnp.dot(row_block, w_value, preferred_element_type=jnp.float32)
    forget_part = jnp.dot(row_block, forget_rows, preferred_element_type=jnp.float32)
    query_sum, key_sum, value_sum, forget_sum = lax.psum(
        (query_part, key_part, value_part, forget_part), "kv"
    )
    first_rms = lax.rsqrt(square_total / full_width + epsilon)[:, None]
    query_local = (query_sum * first_rms).astype(jnp.bfloat16)
    key_new = (key_sum * first_rms).astype(jnp.bfloat16)
    value_new = (value_sum * first_rms).astype(jnp.bfloat16)
    log_gate = jax.nn.log_sigmoid(forget_sum * first_rms + forget_bias)
    query_all = lax.all_gather(query_local, "tp", axis=1, tiled=True)
    batch_rows, key_dims, span = cache_keys.shape
    groups = QUERY_HEAD_COUNT // KV_HEADS
    score_scale = HD ** (-0.5)
    query_grouped = query_all.reshape(batch_rows, KV_HEADS, groups, HD)
    keys_grouped = cache_keys.reshape(batch_rows, KV_HEADS, HD, span)
    values_grouped = cache_values.reshape(batch_rows, KV_HEADS, HD, span)
    scores = jnp.einsum(
        "bkgd,bkdj->bkgj", query_grouped, keys_grouped, preferred_element_type=jnp.float32
    ).reshape(batch_rows, QUERY_HEAD_COUNT, span)
    scores = scores * score_scale + cache_decay + log_gate[:, :, None]
    first_slot = (kv_index * lax.axis_size("tp") + tp_index) * span
    token_positions = first_slot + lax.iota(jnp.int32, span)
    is_live = (token_positions[None, :] < lengths[:, None])[:, None, :]
    scores = jnp.where(is_live, scores, masked_score)
    own_score = (
        jnp.einsum(
            "inpo,ino->inp",
            query_grouped,
            key_new.reshape(batch_rows, KV_HEADS, HD),
            preferred_element_type=jnp.float32,
        ).reshape(batch_rows, QUERY_HEAD_COUNT)
        * score_scale
    )
    local_top = jnp.maximum(jnp.max(scores, axis=2), own_score)
    head_count = w_out.shape[0] // HD
    head_start = tp_index * head_count
    score_top = lax.pmax(local_top, ("kv", "tp"))
    weights = jnp.where(is_live, jnp.exp(scores - score_top[:, :, None]), 0.0)
    weight_total = jnp.sum(weights, axis=2)
    rounded = weights.astype(jnp.bfloat16).reshape(batch_rows, KV_HEADS, groups, span)
    value_sums = jnp.einsum(
        "bkgj,bkdj->bkgd", rounded, values_grouped, preferred_element_type=jnp.float32
    ).reshape(batch_rows, QUERY_HEAD_COUNT, HD)
    weight_total, value_sums = (weight_total, value_sums)
    weight_total, value_sums = (
        lax.psum_scatter(weight_total, "tp", scatter_dimension=1, tiled=True),
        lax.psum_scatter(value_sums, "tp", scatter_dimension=1, tiled=True),
    )
    weight_total, value_sums = lax.psum((weight_total, value_sums), "kv")
    score_top = lax.dynamic_slice_in_dim(score_top, head_start, head_count, 1)
    own_here = lax.dynamic_slice_in_dim(own_score, head_start, head_count, 1)
    new_values = jnp.repeat(value_new.reshape(batch_rows, KV_HEADS, HD), groups, axis=1)
    new_values = lax.dynamic_slice_in_dim(new_values, head_start, head_count, 1).astype(jnp.float32)
    own_weight = jnp.exp(own_here - score_top)
    heads_out = (value_sums + own_weight[:, :, None] * new_values) / (weight_total + own_weight)[
        :, :, None
    ]
    head_gains = lax.dynamic_slice_in_dim(out_gain, head_start * HD, head_count * HD, 0).reshape(
        head_count, HD
    )
    normed = (
        heads_out
        * lax.rsqrt(jnp.mean(jnp.square(heads_out), axis=2, keepdims=True) + epsilon)
        * head_gains
    )
    normed = normed.astype(jnp.bfloat16).reshape(batch_rows, head_count * HD)
    attn_part = jnp.dot(normed, w_out, preferred_element_type=jnp.float32)
    attn_share = lax.psum_scatter(attn_part, "tp", scatter_dimension=1, tiled=True)
    residual = (tokens.astype(jnp.float32) + attn_share).astype(jnp.bfloat16)
    mlp_block, mlp_squares = spread_rows(residual, mlp_gain)
    gate_part = jnp.dot(mlp_block, w_gate, preferred_element_type=jnp.float32)
    up_part = jnp.dot(mlp_block, w_up, preferred_element_type=jnp.float32)
    gate_sum, up_sum = lax.psum((gate_part, up_part), "kv")
    second_rms = lax.rsqrt(mlp_squares / full_width + epsilon)[:, None]
    hidden = (jax.nn.silu(gate_sum * second_rms) * (up_sum * second_rms)).astype(jnp.bfloat16)
    down_part = jnp.dot(hidden, w_down, preferred_element_type=jnp.float32)
    mlp_share = lax.psum_scatter(down_part, "tp", scatter_dimension=1, tiled=True)
    return (residual.astype(jnp.float32) + mlp_share).astype(jnp.bfloat16)


def solution(mesh):
    placed = (
        P(None, ("kv", "tp")),
        P(),
        P(("kv", "tp")),
        P("kv", "tp"),
        P("kv", None),
        P("kv", None),
        P(),
        P(),
        P(None, None, ("kv", "tp")),
        P(None, None, ("kv", "tp")),
        P(None, None, ("kv", "tp")),
        P(),
        P("tp", "kv"),
        P(("kv", "tp")),
        P("kv", "tp"),
        P("kv", "tp"),
        P("tp", "kv"),
    )
    return jax.shard_map(
        body, mesh=mesh, in_specs=placed, out_specs=P(None, ("kv", "tp")), check_vma=False
    )
```

profile of v0, /device:TPU:0, one launch (start us, length us, event | category | flops | bytes accessed | tf_op | source)
XLA Modules:
  0.0 321.7 jit_solution(4829693310829404246)
XLA Ops:
  6.5 0.0 copy-start
  6.5 0.0 copy-start.2
  6.5 0.0 reduce-scatter.9.cloned.1.call-start
  6.5 0.9 dynamic_slice.19
  7.5 0.7 mul.150
  8.2 0.8 fusion.11
  8.9 42.0 %psum.71 = f32[3]{0:T(128)S(1)} all-reduce(f32[3]{0:T(128)S(1)} %get-tuple-element.23), channel_id=1, replica_groups=mesh['kv'=4,'tp'=8] {'kv','tp'}, use_global_device_ids=true, to_apply=%region_2.0 | all-reduce | flops 3 | bytes 24 | tf_op jit(solution)/shard_map/psum | solution.py:17
  51.0 10.6 %all_gather.9 = bf16[3,1024]{1,0:T(4,128)(2,1)S(1)} all-gather(bf16[3,128]{1,0:T(4,128)(2,1)S(1)} %get-tuple-element.24), channel_id=1, replica_groups=mesh['kv'=4,'tp'=8] {'tp'}, dimensions={1}, use_global_device_ids=true | all-gather | bytes 6912 | tf_op jit(solution)/shard_map/all_gather | solution.py:16
  61.5 1.7 fusion.25
  63.2 1.1 fusion.22
  64.3 1.2 fusion.21
  65.5 1.0 fusion.3
  66.5 9.9 %all-reduce.5 = (f32[3,256]{1,0:T(4,128)S(1)}, f32[3,32]{1,0:T(4,128)S(1)}, f32[3,128]{1,0:T(4,128)S(1)}) all-reduce(f32[3,256]{1,0:T(4,128)S(1)} %fusion.21, f32[3,32]{1,0:T(4,128)S(1)} %fusion.3, f32[3,128]{1,0:T(4,128)S(1)} %fusion.22), channel_id=1, replica_groups=mesh['kv'=4,'tp'=8] {'kv'}, use_global_device_ids=true, to_apply=%region_0.0 | all-reduce | flops 1248 | bytes 9984 | tf_op jit(solution)/shard_map/psum | solution.py:50
  76.4 0.1 multiply_convert_fusion.1
  76.5 0.1 multiply_convert_fusion.3
  76.5 0.1 reshape.90
  76.6 12.8 %all_gather.10 = bf16[3,2048]{1,0:T(4,128)(2,1)S(1)} all-gather(bf16[3,256]{1,0:T(4,128)(2,1)S(1)} %multiply_convert_fusion.1), channel_id=1, replica_groups=mesh['kv'=4,'tp'=8] {'tp'}, dimensions={1}, use_global_device_ids=true | all-gather | bytes 13824 | tf_op jit(solution)/shard_map/all_gather | solution.py:58
  89.4 0.1 reshape.78
  89.5 0.1 fusion.23
  89.6 0.1 mul.142
  89.7 0.0 copy-start.3
  89.7 1.1 convolution_multiply_fusion
  90.8 0.7 broadcast_compare_fusion
  91.5 0.0 copy-start.4
  91.5 0.0 copy-done.5
  91.5 0.7 fusion.16
  92.2 1.0 fusion
  93.2 0.0 copy-done.4
  93.2 0.1 select_reduce_fusion
  93.4 0.0 copy-done.3
  93.4 37.8 %pmax.7 = f32[3,32]{1,0:T(4,128)} all-reduce(f32[3,32]{1,0:T(4,128)S(1)} %max.17), channel_id=1, replica_groups=mesh['kv'=4,'tp'=8] {'kv','tp'}, use_global_device_ids=true, to_apply=%region_6.7 | all-reduce | flops 96 | bytes 768 | tf_op jit(solution)/shard_map/pmax | solution.py:85
  131.2 1.4 fusion.1
  132.6 1.2 dynamic-slice
  134.5 1.1 fusion.24
  135.6 27.4 %all-reduce.2 = (f32[3,32,64]{2,1,0:T(8,128)S(1)}, f32[3,32]{1,0:T(4,128)S(1)}) all-reduce(f32[3,32,64]{2,1,0:T(8,128)S(1)} %bitcast.42, f32[3,32]{1,0:T(4,128)} %get-tuple-element.21), channel_id=2, replica_groups=mesh['kv'=4,'tp'=8] {'tp'}, use_global_device_ids=true, to_apply=%region_7.8.clone | all-reduce | flops 6240 | bytes 49920
  163.0 0.1 constant_dynamic-slice_fusion
  163.1 16.6 %all-reduce.4 = (f32[3,4,64]{2,1,0:T(4,128)S(1)}, f32[3,4]{1,0:T(4,128)S(1)}, f32[3,128]{1,0:T(4,128)S(1)}) all-reduce(f32[3,4,64]{2,1,0:T(4,128)S(1)} %constant_dynamic-slice_fusion.1, f32[3,4]{1,0:T(4,128)S(1)} %constant_dynamic-slice_fusion, f32[3,128]{1,0:T(4,128)} %fusion.25), channel_id=1, replica_groups=mesh['kv'=4,'tp'=8] {'kv'}, use_global_device_ids=true, to_apply=%region_8.9 | all-reduce | flops 1164 | bytes 9312 | tf_op jit(solution)/shard_map/psum | solution.py:97
  179.7 0.7 multiply_convert_fusion.2
  180.4 0.1 reshape.84
  180.5 0.8 fusion.20
  181.2 0.2 multiply_reduce_fusion
  181.4 0.8 multiply_convert_fusion
  182.2 0.1 reshape.86
  182.2 0.0 copy-done.2
  182.3 1.1 convolution_bitcast_fusion.1
  183.4 0.0 reduce-scatter.9.cloned.1.call-update
  183.4 0.0 reduce-scatter.11.cloned.1.call-start
  183.5 27.8 %reduce-scatter.9.cloned.1.call-done = f32[128,3]{1,0:T(8,128)} async-done(((f32[1024,3]{1,0:T(8,128)}), f32[128,3]{1,0:T(8,128)}) %reduce-scatter.9.cloned.1.call-update) | async-done | bytes 1552
  211.3 0.9 copy.24
  212.2 0.8 fusion.14
  213.0 37.8 %psum.78 = f32[3]{0:T(128)S(1)} all-reduce(f32[3]{0:T(128)S(1)} %get-tuple-element.15), channel_id=1, replica_groups=mesh['kv'=4,'tp'=8] {'kv','tp'}, use_global_device_ids=true, to_apply=%region_17.18 | all-reduce | flops 3 | bytes 24 | tf_op jit(solution)/shard_map/psum | solution.py:17
  250.8 0.0 copy-start.1
  250.8 0.8 fusion.13
  251.6 11.4 %all_gather.11 = bf16[3,1024]{1,0:T(4,128)(2,1)S(1)} all-gather(bf16[3,128]{1,0:T(4,128)(2,1)S(1)} %fusion.13), channel_id=1, replica_groups=mesh['kv'=4,'tp'=8] {'tp'}, dimensions={1}, use_global_device_ids=true | all-gather | bytes 6912 | tf_op jit(solution)/shard_map/all_gather | solution.py:16
  263.0 0.0 copy-done
  263.0 0.5 fusion.27
  263.5 0.0 copy-done.1
  263.5 0.5 fusion.26
  264.0 16.7 %all-reduce.3 = (f32[3,1408]{1,0:T(4,128)S(1)}, f32[3,1408]{1,0:T(4,128)S(1)}) all-reduce(f32[3,1408]{1,0:T(4,128)S(1)} %fusion.27, f32[3,1408]{1,0:T(4,128)S(1)} %fusion.26), channel_id=1, replica_groups=mesh['kv'=4,'tp'=8] {'kv'}, use_global_device_ids=true, to_apply=%region_18.19 | all-reduce | flops 8448 | bytes 67584 | tf_op jit(solution)/shard_map/psum | solution.py:121
  280.7 3.8 %convolution_bitcast_fusion = f32[1024,3]{1,0:T(8,128)} fusion(bf16[1408,1024]{1,0:T(8,128)(2,1)} %param.33, f32[3,1408]{1,0:T(4,128)S(1)} %get-tuple-element.7, f32[3,1408]{1,0:T(4,128)S(1)} %get-tuple-element.8, f32[3]{0:T(128)S(1)} %add_rsqrt_fusion.1), kind=kOutput, calls=%fused_computation | convolution fusion | flops 8684544 | bytes 2929676
  284.5 0.0 reduce-scatter.11.cloned.1.call-update
  284.5 28.8 %reduce-scatter.11.cloned.1.call-done = f32[128,3]{1,0:T(8,128)} async-done(((f32[1024,3]{1,0:T(8,128)}), f32[128,3]{1,0:T(8,128)}) %reduce-scatter.11.cloned.1.call-update) | async-done | bytes 1552
  313.3 0.9 copy.26
  314.2 0.6 fusion.15
  (9 shorter events, 0.1 us)
Async XLA Ops:
  6.5 256.5 %copy-start = (bf16[1024,1408]{1,0:T(8,128)(2,1)S(1)}, bf16[1024,1408]{1,0:T(8,128)(2,1)}, u32[]{:S(2)}) copy-start(bf16[1024,1408]{1,0:T(8,128)(2,1)} %param.32) | copy-start | bytes 8650756
  6.5 175.7 %copy-start.2 = (bf16[256,1024]{1,0:T(8,128)(2,1)S(1)}, bf16[256,1024]{1,0:T(8,128)(2,1)}, u32[]{:S(2)}) copy-start(bf16[256,1024]{1,0:T(8,128)(2,1)} %param.29) | copy-start | bytes 1572868
  6.5 204.8 %reduce-scatter.9.cloned.1.call-start = ((), (), s32[]{:S(2)}) async-start(), calls=%async_computation.2 | async-start | bytes 589824
  50.9 40.6 %copy-start.5 = (f32[3]{0:T(128)}, f32[3]{0:T(128)S(1)}, u32[]{:S(2)}) copy-start(f32[3]{0:T(128)S(1)} %add_rsqrt_fusion.2) | copy-start | bytes 40
  89.7 3.7 %copy-start.3 = (f32[3,32]{1,0:T(4,128)}, f32[3,32]{1,0:T(4,128)S(1)}, u32[]{:S(2)}) copy-start(f32[3,32]{1,0:T(4,128)S(1)} %mul.142) | copy-start | bytes 1156
  91.5 1.7 copy-start.4
  183.4 129.9 %reduce-scatter.11.cloned.1.call-start = ((), (), s32[]{:S(2)}) async-start(), calls=%async_computation.3 | async-start | bytes 589824
  250.8 12.7 %copy-start.1 = (bf16[1024,1408]{1,0:T(8,128)(2,1)S(1)}, bf16[1024,1408]{1,0:T(8,128)(2,1)}, u32[]{:S(2)}) copy-start(bf16[1024,1408]{1,0:T(8,128)(2,1)} %param.31) | copy-start | bytes 8650756
Sparse Core Ops, SparseCore 0:
  183.5 27.7 reduce-scatter.8
  284.6 28.6 reduce-scatter.10
where the time goes:
time: 323 us; the launch traced here: 322 us
  blocking collectives  223 us (69%)
  waiting for transfers between devices  56.7 us (18%)
  between operations  14.1 us (4%)
  matrix products  13.2 us (4%)
  other arithmetic  9.52 us (3%)
  local copies, waits for them, and re-layouts  5.19 us (2%)
    psum x2, blocking collectives, spread_rows(): square_total = lax.psum(squares, ('kv', 'tp'))  79.8 us
    unnamed x4, waiting for transfers between devices  56.7 us
    pmax x1, blocking collectives, body(): score_top = lax.pmax(local_top, ('kv', 'tp'))  37.8 us
    unnamed x1, blocking collectives  27.4 us
    all_gather x2, blocking collectives, spread_rows(): row_block = lax.all_gather(scaled, 'tp', axis=1, tiled=True)  22 us
    psum x1, blocking collectives, body(): gate_sum, up_sum = lax.psum((gate_part, up_part), 'kv')  16.7 us
    psum x1, blocking collectives, body(): weight_total, value_sums = lax.psum((weight_total, value_sums), 'kv')  16.6 us
    all_gather x1, blocking collectives, body(): query_all = lax.all_gather(query_local, 'tp', axis=1, tiled=True)  12.8 us
  transfers between devices with their start and end apart: 2, of which 2 were waited for; matrix products, arithmetic and copies ran while one was open for 0% of the time, Pallas kernels for 0%

commit v1 on v0

--- a/solution.py
+++ b/solution.py
@@ -10,10 +10,28 @@
 masked_score = -1e30
 
 
+def zones_scan(vals, d_out):
+    which_axis = "tp"
+    n_parts = lax.axis_size(which_axis)
+    kept_rows = [(dev_j, (dev_j + 1) % n_parts) for dev_j in range(n_parts)]
+
+    def _solve_tables(known):
+        if len(known) == n_parts:
+            return known
+        q_next = lax.ppermute(known[0], axis_name=which_axis, perm=kept_rows)
+        upper = _solve_tables([q_next, *known])
+        return upper
+
+    taken_in = _solve_tables([vals])
+    built = jnp.concatenate(taken_in, axis=d_out)
+    odd = jnp.roll(built, (lax.axis_index(which_axis) + 1) * vals.shape[d_out], axis=d_out)
+    return odd
+
+
 def spread_rows(share, gain):
     scaled = (share.astype(jnp.float32) * gain).astype(jnp.bfloat16)
     squares = jnp.sum(jnp.square(share.astype(jnp.float32)), axis=1)
-    row_block = lax.all_gather(scaled, "tp", axis=1, tiled=True)
+    row_block = zones_scan(scaled, d_out=1)
     square_total = lax.psum(squares, ("kv", "tp"))
     return (row_block, square_total)
 

time: 323 us -> 350 us (1.084)
  waiting for transfers between devices: 56.7 us -> 111 us
  blocking collectives: 223 us -> 200 us
  other arithmetic: 9.52 us -> 5.02 us
    ppermute x0 -> x14, waiting for transfers between devices: none -> 55.2 us  [_solve_tables(): q_next = lax.ppermute(known[0], axis_name=which_axis, perm=kept_rows)]
    all_gather x2 -> x0, blocking collectives: 22 us -> none  [spread_rows(): row_block = lax.all_gather(scaled, 'tp', axis=1, tiled=True)]
  transfers between devices with their start and end apart: 2 -> 16, of which waited for: 2 -> 14; matrix products, arithmetic and copies ran while one was open for 0% -> 1% of each run, Pallas kernels for 0% -> 0%
where the time goes in v1:
time: 350 us
  blocking collectives  200 us (57%)
  waiting for transfers between devices  111 us (32%)
  between operations  14.2 us (4%)
  matrix products  12.7 us (4%)
  local copies, waits for them, and re-layouts  5.23 us (1%)
  other arithmetic  5.02 us (1%)
    psum x2, blocking collectives, spread_rows(): square_total = lax.psum(squares, ('kv', 'tp'))  78.1 us
    unnamed x4, waiting for transfers between devices  56.1 us
    ppermute x14, waiting for transfers between devices, _solve_tables(): q_next = lax.ppermute(known[0], axis_name=which_axis, perm=kept_rows)  55.2 us
    pmax x1, blocking collectives, body(): score_top = lax.pmax(local_top, ('kv', 'tp'))  37.8 us
    unnamed x1, blocking collectives  27.8 us
    psum x1, blocking collectives, body(): gate_sum, up_sum = lax.psum((gate_part, up_part), 'kv')  17.3 us
    psum x1, blocking collectives, body(): weight_total, value_sums = lax.psum((weight_total, value_sums), 'kv')  15.8 us
    all_gather x1, blocking collectives, body(): query_all = lax.all_gather(query_local, 'tp', axis=1, tiled=True)  12.8 us
  transfers between devices with their start and end apart: 16, of which 14 were waited for; matrix products, arithmetic and copies ran while one was open for 1% of the time, Pallas kernels for 0%

profile of v1, /device:TPU:0, one launch (start us, length us, event | category | flops | bytes accessed | tf_op | source)
XLA Modules:
  0.0 349.7 jit_solution(16582781418389402827)
XLA Ops:
  6.5 0.0 reduce-scatter.9.cloned.1.call-start
  6.6 1.0 fusion.13
  7.6 0.5 collective-permute-start
  8.1 5.3 %collective-permute-done = bf16[3,128]{1,0:T(4,128)(2,1)S(1)} collective-permute-done((bf16[3,128]{1,0:T(4,128)(2,1)S(1)}, bf16[3,128]{1,0:T(4,128)(2,1)S(1)}, u32[]{:S(2)}, u32[]{:S(2)}) %collective-permute-start) | collective-permute-done | bytes 800 | tf_op jit(solution)/shard_map/ppermute | solution.py:21
  13.4 4.8 %collective-permute-done.1 = bf16[3,128]{1,0:T(4,128)(2,1)S(1)} collective-permute-done((bf16[3,128]{1,0:T(4,128)(2,1)S(1)}, bf16[3,128]{1,0:T(4,128)(2,1)S(1)}, u32[]{:S(2)}, u32[]{:S(2)}) %collective-permute-start.1) | collective-permute-done | bytes 800 | tf_op jit(solution)/shard_map/ppermute | solution.py:21
  18.2 0.7 broadcast_compare_fusion
  18.9 39.3 %psum.71 = f32[3]{0:T(128)S(1)} all-reduce(f32[3]{0:T(128)S(1)} %get-tuple-element.24), channel_id=1, replica_groups=mesh['kv'=4,'tp'=8] {'kv','tp'}, use_global_device_ids=true, to_apply=%region_2.4 | all-reduce | flops 3 | bytes 24 | tf_op jit(solution)/shard_map/psum | solution.py:35
  58.2 4.8 %collective-permute-done.3 = bf16[3,128]{1,0:T(4,128)(2,1)S(1)} collective-permute-done((bf16[3,128]{1,0:T(4,128)(2,1)S(1)}, bf16[3,128]{1,0:T(4,128)(2,1)S(1)}, u32[]{:S(2)}, u32[]{:S(2)}) %collective-permute-start.3) | collective-permute-done | bytes 800 | tf_op jit(solution)/shard_map/ppermute | solution.py:21
  63.0 4.8 %collective-permute-done.4 = bf16[3,128]{1,0:T(4,128)(2,1)S(1)} collective-permute-done((bf16[3,128]{1,0:T(4,128)(2,1)S(1)}, bf16[3,128]{1,0:T(4,128)(2,1)S(1)}, u32[]{:S(2)}, u32[]{:S(2)}) %collective-permute-start.4) | collective-permute-done | bytes 800 | tf_op jit(solution)/shard_map/ppermute | solution.py:21
  67.8 4.8 %collective-permute-done.5 = bf16[3,128]{1,0:T(4,128)(2,1)S(1)} collective-permute-done((bf16[3,128]{1,0:T(4,128)(2,1)S(1)}, bf16[3,128]{1,0:T(4,128)(2,1)S(1)}, u32[]{:S(2)}, u32[]{:S(2)}) %collective-permute-start.5) | collective-permute-done | bytes 800 | tf_op jit(solution)/shard_map/ppermute | solution.py:21
  72.6 0.8 dynamic_slice.22
  73.4 0.1 mul.155
  73.4 1.2 dynamic-slice
  75.3 2.1 collective-permute-done.6
  77.5 1.1 fusion.27
  78.6 1.1 fusion.32
  79.7 1.2 fusion.30
  80.9 1.0 fusion.3
  81.9 10.7 %all-reduce.5 = (f32[3,256]{1,0:T(4,128)S(1)}, f32[3,32]{1,0:T(4,128)S(1)}, f32[3,128]{1,0:T(4,128)S(1)}) all-reduce(f32[3,256]{1,0:T(4,128)S(1)} %fusion.30, f32[3,32]{1,0:T(4,128)S(1)} %fusion.3, f32[3,128]{1,0:T(4,128)S(1)} %fusion.27), channel_id=1, replica_groups=mesh['kv'=4,'tp'=8] {'kv'}, use_global_device_ids=true, to_apply=%region_0.2 | all-reduce | flops 1248 | bytes 9984 | tf_op jit(solution)/shard_map/psum | solution.py:68
  92.6 0.1 multiply_convert_fusion.1
  92.7 0.1 multiply_convert_fusion.3
  92.8 0.1 reshape.90
  92.9 12.8 %all_gather.3 = bf16[3,2048]{1,0:T(4,128)(2,1)S(1)} all-gather(bf16[3,256]{1,0:T(4,128)(2,1)S(1)} %multiply_convert_fusion.1), channel_id=1, replica_groups=mesh['kv'=4,'tp'=8] {'tp'}, dimensions={1}, use_global_device_ids=true | all-gather | bytes 13824 | tf_op jit(solution)/shard_map/all_gather | solution.py:76
  105.6 0.1 reshape.78
  105.7 0.1 fusion.34
  105.9 0.1 mul.147
  106.0 1.1 convolution_multiply_fusion
  107.0 0.7 fusion.18
  107.8 1.0 fusion
  108.8 0.1 select_reduce_fusion
  108.9 37.8 %pmax.7 = f32[3,32]{1,0:T(4,128)S(1)} all-reduce(f32[3,32]{1,0:T(4,128)S(1)} %max.17), channel_id=1, replica_groups=mesh['kv'=4,'tp'=8] {'kv','tp'}, use_global_device_ids=true, to_apply=%region_6.8 | all-reduce | flops 96 | bytes 768 | tf_op jit(solution)/shard_map/pmax | solution.py:103
  146.7 0.2 fusion.1
  146.9 1.1 fusion.35
  147.9 27.8 %all-reduce.2 = (f32[3,32,64]{2,1,0:T(8,128)}, f32[3,32]{1,0:T(4,128)S(1)}) all-reduce(f32[3,32,64]{2,1,0:T(8,128)S(1)} %bitcast.36, f32[3,32]{1,0:T(4,128)S(1)} %get-tuple-element.22), channel_id=2, replica_groups=mesh['kv'=4,'tp'=8] {'tp'}, use_global_device_ids=true, to_apply=%region_7.9.clone | all-reduce | flops 6240 | bytes 49920
  175.8 0.7 constant_dynamic-slice_fusion.1
  176.5 0.1 constant_dynamic-slice_fusion
  176.5 15.8 %all-reduce.4 = (f32[3,4,64]{2,1,0:T(4,128)S(1)}, f32[3,4]{1,0:T(4,128)S(1)}, f32[3,128]{1,0:T(4,128)S(1)}) all-reduce(f32[3,4,64]{2,1,0:T(4,128)S(1)} %constant_dynamic-slice_fusion.1, f32[3,4]{1,0:T(4,128)S(1)} %constant_dynamic-slice_fusion, f32[3,128]{1,0:T(4,128)S(1)} %fusion.32), channel_id=1, replica_groups=mesh['kv'=4,'tp'=8] {'kv'}, use_global_device_ids=true, to_apply=%region_8.10 | all-reduce | flops 1164 | bytes 9312 | tf_op jit(solution)/shard_map/psum | solution.py:115
  192.4 0.1 multiply_convert_fusion.2
  192.4 0.1 reshape.84
  192.5 0.1 fusion.26
  192.6 0.2 multiply_reduce_fusion
  192.8 0.1 multiply_convert_fusion
  192.9 0.1 reshape.86
  193.0 1.1 convolution_bitcast_fusion.1
  194.1 0.0 reduce-scatter.11.cloned.1.call-start
  194.2 27.7 %reduce-scatter.9.cloned.1.call-done = f32[128,3]{1,0:T(8,128)} async-done(((f32[1024,3]{1,0:T(8,128)}), f32[128,3]{1,0:T(8,128)}) %reduce-scatter.9.cloned.1.call-update) | async-done | bytes 1552
  221.9 0.9 copy.24
  222.8 0.1 fusion.16
  223.0 0.1 collective-permute-start.7
  223.0 4.8 %collective-permute-done.7 = bf16[3,128]{1,0:T(4,128)(2,1)S(1)} collective-permute-done((bf16[3,128]{1,0:T(4,128)(2,1)S(1)}, bf16[3,128]{1,0:T(4,128)(2,1)S(1)}, u32[]{:S(2)}, u32[]{:S(2)}) %collective-permute-start.7) | collective-permute-done | bytes 800 | tf_op jit(solution)/shard_map/ppermute | solution.py:21
  227.8 4.8 %collective-permute-done.8 = bf16[3,128]{1,0:T(4,128)(2,1)S(1)} collective-permute-done((bf16[3,128]{1,0:T(4,128)(2,1)S(1)}, bf16[3,128]{1,0:T(4,128)(2,1)S(1)}, u32[]{:S(2)}, u32[]{:S(2)}) %collective-permute-start.8) | collective-permute-done | bytes 800 | tf_op jit(solution)/shard_map/ppermute | solution.py:21
  232.6 4.8 %collective-permute-done.9 = bf16[3,128]{1,0:T(4,128)(2,1)S(1)} collective-permute-done((bf16[3,128]{1,0:T(4,128)(2,1)S(1)}, bf16[3,128]{1,0:T(4,128)(2,1)S(1)}, u32[]{:S(2)}, u32[]{:S(2)}) %collective-permute-start.9) | collective-permute-done | bytes 800 | tf_op jit(solution)/shard_map/ppermute | solution.py:21
  237.4 4.8 %collective-permute-done.10 = bf16[3,128]{1,0:T(4,128)(2,1)S(1)} collective-permute-done((bf16[3,128]{1,0:T(4,128)(2,1)S(1)}, bf16[3,128]{1,0:T(4,128)(2,1)S(1)}, u32[]{:S(2)}, u32[]{:S(2)}) %collective-permute-start.10) | collective-permute-done | bytes 800 | tf_op jit(solution)/shard_map/ppermute | solution.py:21
  242.2 4.8 %collective-permute-done.11 = bf16[3,128]{1,0:T(4,128)(2,1)S(1)} collective-permute-done((bf16[3,128]{1,0:T(4,128)(2,1)S(1)}, bf16[3,128]{1,0:T(4,128)(2,1)S(1)}, u32[]{:S(2)}, u32[]{:S(2)}) %collective-permute-start.11) | collective-permute-done | bytes 800 | tf_op jit(solution)/shard_map/ppermute | solution.py:21
  247.0 38.8 %psum.78 = f32[3]{0:T(128)S(1)} all-reduce(f32[3]{0:T(128)S(1)} %get-tuple-element.16), channel_id=1, replica_groups=mesh['kv'=4,'tp'=8] {'kv','tp'}, use_global_device_ids=true, to_apply=%region_17.19 | all-reduce | flops 3 | bytes 24 | tf_op jit(solution)/shard_map/psum | solution.py:35
  285.8 0.0 collective-permute-start.13
  285.9 4.8 %collective-permute-done.13 = bf16[3,128]{1,0:T(4,128)(2,1)S(1)} collective-permute-done((bf16[3,128]{1,0:T(4,128)(2,1)S(1)}, bf16[3,128]{1,0:T(4,128)(2,1)S(1)}, u32[]{:S(2)}, u32[]{:S(2)}) %collective-permute-start.13) | collective-permute-done | bytes 800 | tf_op jit(solution)/shard_map/ppermute | solution.py:21
  290.8 0.5 fusion.21
  291.2 0.5 fusion.23
  291.7 17.3 %all-reduce.3 = (f32[3,1408]{1,0:T(4,128)S(1)}, f32[3,1408]{1,0:T(4,128)S(1)}) all-reduce(f32[3,1408]{1,0:T(4,128)S(1)} %fusion.23, f32[3,1408]{1,0:T(4,128)S(1)} %fusion.21), channel_id=1, replica_groups=mesh['kv'=4,'tp'=8] {'kv'}, use_global_device_ids=true, to_apply=%region_18.20 | all-reduce | flops 8448 | bytes 67584 | tf_op jit(solution)/shard_map/psum | solution.py:139
  309.1 3.8 %convolution_bitcast_fusion = f32[1024,3]{1,0:T(8,128)} fusion(bf16[1408,1024]{1,0:T(8,128)(2,1)} %param.35, f32[3,1408]{1,0:T(4,128)S(1)} %get-tuple-element.8, f32[3,1408]{1,0:T(4,128)S(1)} %get-tuple-element.9, f32[3]{0:T(128)S(1)} %add_rsqrt_fusion.1), kind=kOutput, calls=%fused_computation | convolution fusion | flops 8684544 | bytes 2929676
  312.9 28.4 %reduce-scatter.11.cloned.1.call-done = f32[128,3]{1,0:T(8,128)} async-done(((f32[1024,3]{1,0:T(8,128)}), f32[128,3]{1,0:T(8,128)}) %reduce-scatter.11.cloned.1.call-update) | async-done | bytes 1552
  341.3 0.9 copy.26
  342.2 0.6 fusion.17
  (49 shorter events, 0.3 us)
Async XLA Ops:
  6.5 284.2 %copy-start = (bf16[1024,1408]{1,0:T(8,128)(2,1)S(1)}, bf16[1024,1408]{1,0:T(8,128)(2,1)}, u32[]{:S(2)}) copy-start(bf16[1024,1408]{1,0:T(8,128)(2,1)} %param.33) | copy-start | bytes 8650756
  6.5 216.3 %copy-start.3 = (bf16[3,128]{1,0:T(4,128)(2,1)S(1)}, bf16[3,128]{1,0:T(4,128)(2,1)}, u32[]{:S(2)}) copy-start(bf16[3,128]{1,0:T(4,128)(2,1)} %param.19) | copy-start | bytes 2308
  6.5 186.4 %copy-start.2 = (bf16[256,1024]{1,0:T(8,128)(2,1)S(1)}, bf16[256,1024]{1,0:T(8,128)(2,1)}, u32[]{:S(2)}) copy-start(bf16[256,1024]{1,0:T(8,128)(2,1)} %param.31) | copy-start | bytes 1572868
  6.5 216.4 %copy-start.4 = (f32[128]{0:T(128)S(1)}, f32[128]{0:T(128)}, u32[]{:S(2)}) copy-start(f32[128]{0:T(128)} %param.32) | copy-start | bytes 1540
  6.5 215.4 %reduce-scatter.9.cloned.1.call-start = ((), (), s32[]{:S(2)}) async-start(), calls=%async_computation.2 | async-start | bytes 589824
  7.6 5.8 %collective-permute-start = (bf16[3,128]{1,0:T(4,128)(2,1)S(1)}, bf16[3,128]{1,0:T(4,128)(2,1)S(1)}, u32[]{:S(2)}, u32[]{:S(2)}) collective-permute-start(bf16[3,128]{1,0:T(4,128)(2,1)S(1)} %get-tuple-element.25), channel_id=1, source_target_pairs={{0,1},{1,2},{2,3},{3,4},{4,5},{5,6},{6,7},{7,0},{8,9},{9,10},{10,1... | collective-permute-start | bytes 2312 | tf_op jit(solution)/shard_map/ppermute | solution.py:21
  13.4 4.8 %collective-permute-start.1 = (bf16[3,128]{1,0:T(4,128)(2,1)S(1)}, bf16[3,128]{1,0:T(4,128)(2,1)S(1)}, u32[]{:S(2)}, u32[]{:S(2)}) collective-permute-start(bf16[3,128]{1,0:T(4,128)(2,1)S(1)} %collective-permute-done), channel_id=1, source_target_pairs={{0,1},{1,2},{2,3},{3,4},{4,5},{5,6},{6,7},{7,0},{8,9},{9,10},{10,1... | collective-permute-start | bytes 2312 | tf_op jit(solution)/shard_map/ppermute | solution.py:21
  18.2 40.0 %collective-permute-start.2 = (bf16[3,128]{1,0:T(4,128)(2,1)S(1)}, bf16[3,128]{1,0:T(4,128)(2,1)S(1)}, u32[]{:S(2)}, u32[]{:S(2)}) collective-permute-start(bf16[3,128]{1,0:T(4,128)(2,1)S(1)} %collective-permute-done.1), channel_id=1, source_target_pairs={{0,1},{1,2},{2,3},{3,4},{4,5},{5,6},{6,7},{7,0},{8,9},{9,10},{10,1... | collective-permute-start | bytes 2312 | tf_op jit(solution)/shard_map/ppermute | solution.py:21
  58.2 4.8 %collective-permute-start.3 = (bf16[3,128]{1,0:T(4,128)(2,1)S(1)}, bf16[3,128]{1,0:T(4,128)(2,1)S(1)}, u32[]{:S(2)}, u32[]{:S(2)}) collective-permute-start(bf16[3,128]{1,0:T(4,128)(2,1)S(1)} %collective-permute-done.2), channel_id=1, source_target_pairs={{0,1},{1,2},{2,3},{3,4},{4,5},{5,6},{6,7},{7,0},{8,9},{9,10},{10,1... | collective-permute-start | bytes 2312 | tf_op jit(solution)/shard_map/ppermute | solution.py:21
  63.0 4.8 %collective-permute-start.4 = (bf16[3,128]{1,0:T(4,128)(2,1)S(1)}, bf16[3,128]{1,0:T(4,128)(2,1)S(1)}, u32[]{:S(2)}, u32[]{:S(2)}) collective-permute-start(bf16[3,128]{1,0:T(4,128)(2,1)S(1)} %collective-permute-done.3), channel_id=1, source_target_pairs={{0,1},{1,2},{2,3},{3,4},{4,5},{5,6},{6,7},{7,0},{8,9},{9,10},{10,1... | collective-permute-start | bytes 2312 | tf_op jit(solution)/shard_map/ppermute | solution.py:21
  67.8 4.8 %collective-permute-start.5 = (bf16[3,128]{1,0:T(4,128)(2,1)S(1)}, bf16[3,128]{1,0:T(4,128)(2,1)S(1)}, u32[]{:S(2)}, u32[]{:S(2)}) collective-permute-start(bf16[3,128]{1,0:T(4,128)(2,1)S(1)} %collective-permute-done.4), channel_id=1, source_target_pairs={{0,1},{1,2},{2,3},{3,4},{4,5},{5,6},{6,7},{7,0},{8,9},{9,10},{10,1... | collective-permute-start | bytes 2312 | tf_op jit(solution)/shard_map/ppermute | solution.py:21
  72.6 4.8 %collective-permute-start.6 = (bf16[3,128]{1,0:T(4,128)(2,1)S(1)}, bf16[3,128]{1,0:T(4,128)(2,1)S(1)}, u32[]{:S(2)}, u32[]{:S(2)}) collective-permute-start(bf16[3,128]{1,0:T(4,128)(2,1)S(1)} %collective-permute-done.5), channel_id=1, source_target_pairs={{0,1},{1,2},{2,3},{3,4},{4,5},{5,6},{6,7},{7,0},{8,9},{9,10},{10,1... | collective-permute-start | bytes 2312 | tf_op jit(solution)/shard_map/ppermute | solution.py:21
  194.1 147.2 %reduce-scatter.11.cloned.1.call-start = ((), (), s32[]{:S(2)}) async-start(), calls=%async_computation.3 | async-start | bytes 589824
  223.0 4.8 %collective-permute-start.7 = (bf16[3,128]{1,0:T(4,128)(2,1)S(1)}, bf16[3,128]{1,0:T(4,128)(2,1)S(1)}, u32[]{:S(2)}, u32[]{:S(2)}) collective-permute-start(bf16[3,128]{1,0:T(4,128)(2,1)S(1)} %fusion.15), channel_id=1, source_target_pairs={{0,1},{1,2},{2,3},{3,4},{4,5},{5,6},{6,7},{7,0},{8,9},{9,10},{10,1... | collective-permute-start | bytes 2312 | tf_op jit(solution)/shard_map/ppermute | solution.py:21
  227.8 4.8 %collective-permute-start.8 = (bf16[3,128]{1,0:T(4,128)(2,1)S(1)}, bf16[3,128]{1,0:T(4,128)(2,1)S(1)}, u32[]{:S(2)}, u32[]{:S(2)}) collective-permute-start(bf16[3,128]{1,0:T(4,128)(2,1)S(1)} %collective-permute-done.7), channel_id=1, source_target_pairs={{0,1},{1,2},{2,3},{3,4},{4,5},{5,6},{6,7},{7,0},{8,9},{9,10},{10,1... | collective-permute-start | bytes 2312 | tf_op jit(solution)/shard_map/ppermute | solution.py:21
  232.6 4.8 %collective-permute-start.9 = (bf16[3,128]{1,0:T(4,128)(2,1)S(1)}, bf16[3,128]{1,0:T(4,128)(2,1)S(1)}, u32[]{:S(2)}, u32[]{:S(2)}) collective-permute-start(bf16[3,128]{1,0:T(4,128)(2,1)S(1)} %collective-permute-done.8), channel_id=1, source_target_pairs={{0,1},{1,2},{2,3},{3,4},{4,5},{5,6},{6,7},{7,0},{8,9},{9,10},{10,1... | collective-permute-start | bytes 2312 | tf_op jit(solution)/shard_map/ppermute | solution.py:21
  237.4 4.8 %collective-permute-start.10 = (bf16[3,128]{1,0:T(4,128)(2,1)S(1)}, bf16[3,128]{1,0:T(4,128)(2,1)S(1)}, u32[]{:S(2)}, u32[]{:S(2)}) collective-permute-start(bf16[3,128]{1,0:T(4,128)(2,1)S(1)} %collective-permute-done.9), channel_id=1, source_target_pairs={{0,1},{1,2},{2,3},{3,4},{4,5},{5,6},{6,7},{7,0},{8,9},{9,10},{10,1... | collective-permute-start | bytes 2312 | tf_op jit(solution)/shard_map/ppermute | solution.py:21
  242.2 4.8 %collective-permute-start.11 = (bf16[3,128]{1,0:T(4,128)(2,1)S(1)}, bf16[3,128]{1,0:T(4,128)(2,1)S(1)}, u32[]{:S(2)}, u32[]{:S(2)}) collective-permute-start(bf16[3,128]{1,0:T(4,128)(2,1)S(1)} %collective-permute-done.10), channel_id=1, source_target_pairs={{0,1},{1,2},{2,3},{3,4},{4,5},{5,6},{6,7},{7,0},{8,9},{9,10},{10,1... | collective-permute-start | bytes 2312 | tf_op jit(solution)/shard_map/ppermute | solution.py:21
  247.0 38.8 %collective-permute-start.12 = (bf16[3,128]{1,0:T(4,128)(2,1)S(1)}, bf16[3,128]{1,0:T(4,128)(2,1)S(1)}, u32[]{:S(2)}, u32[]{:S(2)}) collective-permute-start(bf16[3,128]{1,0:T(4,128)(2,1)S(1)} %collective-permute-done.11), channel_id=1, source_target_pairs={{0,1},{1,2},{2,3},{3,4},{4,5},{5,6},{6,7},{7,0},{8,9},{9,10},{10,1... | collective-permute-start | bytes 2312 | tf_op jit(solution)/shard_map/ppermute | solution.py:21
  285.8 5.4 %copy-start.1 = (bf16[1024,1408]{1,0:T(8,128)(2,1)S(1)}, bf16[1024,1408]{1,0:T(8,128)(2,1)}, u32[]{:S(2)}) copy-start(bf16[1024,1408]{1,0:T(8,128)(2,1)} %param.34) | copy-start | bytes 8650756
  285.8 4.8 %collective-permute-start.13 = (bf16[3,128]{1,0:T(4,128)(2,1)S(1)}, bf16[3,128]{1,0:T(4,128)(2,1)S(1)}, u32[]{:S(2)}, u32[]{:S(2)}) collective-permute-start(bf16[3,128]{1,0:T(4,128)(2,1)S(1)} %collective-permute-done.12), channel_id=1, source_target_pairs={{0,1},{1,2},{2,3},{3,4},{4,5},{5,6},{6,7},{7,0},{8,9},{9,10},{10,1... | collective-permute-start | bytes 2312 | tf_op jit(solution)/shard_map/ppermute | solution.py:21
Sparse Core Ops, SparseCore 0:
  194.2 27.6 reduce-scatter.8
  313.1 28.2 reduce-scatter.10
